TPU v7x, 512 devices: a whole 4x4x16 slice. The times are simulated.
512 devices in a mesh: ra: 16 (over z), cb: 4 (over y), dp: 8 (over x, core).
Axes of the slice: x: 4, y: 4, z: 16, core: 2. Of those that a mesh axis runs over, the one named last changes fastest.
Arguments:
- tokens: bfloat16 [8, 512, 4096], P('dp', None, 'ra'), may hold values from -80 to 80
- pre_gain: float32 [4096], P('ra'), may hold values from 0.1 to 1.9
- w_gate: bfloat16 [4096, 11264], P('ra', 'cb'), may hold values from -0.09375 to 0.09375
- w_up: bfloat16 [4096, 11264], P('ra', 'cb'), may hold values from -0.09375 to 0.09375
- conv_gate: float32 [3, 11264], P(None, 'cb'), may hold values from -3.5 to 3.5
- conv_up: float32 [3, 11264], P(None, 'cb'), may hold values from -3.5 to 3.5
- w_down: bfloat16 [11264, 4096], P('cb', 'ra'), may hold values from -2 to 2
- post_gain: float32 [4096], P('ra'), may hold values from 0.1 to 1.9
Outputs:
- mixed: bfloat16 [8, 512, 4096], P('dp', None, 'ra')
All inputs are finite; a program needn't handle non-finite values.
Results may differ from a plain program's by a relative error of at most 0.0064.
Values may be sent and summed in bfloat16 or wider, within the bound.
A program may use at most 64 MiB of HBM per device.

v0:
```python
import jax
import jax.numpy as jnp
from jax import lax
from jax.sharding import PartitionSpec as P

epsilon = 1e-06
residual_scale = 0.125


def from_everyone(array, axis):
    count = lax.axis_size(axis)
    return lax.all_to_all(
        jnp.broadcast_to(array[None], (count, *array.shape)), axis, 0, 0, tiled=True
    )


def over_copies(array, axis):
    return from_everyone(array, axis).sum(axis=0)


def split_up(array, dim, count):
    dims = array.shape
    tiles = array.reshape(*dims[:dim], count, dims[dim] // count, *dims[dim + 1 :])
    return jnp.moveaxis(tiles, dim, 0)


def summed_on_arrival(array, axis, dim):
    count = lax.axis_size(axis)
    tiles = lax.all_to_all(split_up(array, dim, count), axis, 0, 0, tiled=True)
    return jnp.sum(tiles, axis=0)


def convolve(field, tap_weights):
    zero_col = jnp.zeros((field.shape[0], 1), jnp.float32)
    before = jnp.concatenate([zero_col, field[:, :-1]], axis=1)
    later_cols = jnp.concatenate([field[:, 1:], zero_col], axis=1)
    return (
        tap_weights[0][:, None] * before
        + tap_weights[1][:, None] * field
        + tap_weights[2][:, None] * later_cols
    )


def local(tokens, pre_gain, w_gate, w_up, conv_gate, conv_up, w_down, post_gain):
    ra_count = lax.axis_size("ra")
    dim_full = tokens.shape[2] * ra_count
    values = tokens[0].astype(jnp.float32)
    local_sq = jnp.sum(values * values, axis=1)
    total_sq = over_copies(local_sq, "ra")
    in_scale = lax.rsqrt(total_sq / dim_full + epsilon)
    weighted = (values * pre_gain).astype(jnp.bfloat16)
    gate_cols, up_cols = (
        lax.all_to_all(w_gate, "ra", split_axis=1, concat_axis=0, tiled=True),
        lax.all_to_all(w_up, "ra", split_axis=1, concat_axis=0, tiled=True),
    )
    own_units = gate_cols.shape[1]
    piece = lax.all_gather(weighted, "ra", axis=1, tiled=True)
    dims = (((0,), (1,)), ((), ()))
    gate_sum = lax.dot_general(gate_cols, piece, dims, preferred_element_type=jnp.float32)
    up_sum = lax.dot_general(up_cols, piece, dims, preferred_element_type=jnp.float32)
    offset_units = lax.axis_index("ra") * own_units
    taps_gate = lax.dynamic_slice_in_dim(conv_gate, offset_units, own_units, 1)
    taps_up = lax.dynamic_slice_in_dim(conv_up, offset_units, own_units, 1)
    gate_lin = gate_sum * in_scale[None, :]
    up_lin = up_sum * in_scale[None, :]
    hidden = (
        jax.nn.gelu(convolve(gate_lin, taps_gate), approximate=True) * convolve(up_lin, taps_up)
    ).astype(jnp.bfloat16)
    partial_value = lax.dot_general(
        lax.all_gather(hidden, "ra", axis=0, tiled=True),
        w_down,
        (((0,), (0,)), ((), ())),
        preferred_element_type=jnp.float32,
    )
    share = summed_on_arrival(partial_value, "cb", 1)
    share_cols = share.shape[1]
    col_start = lax.axis_index("cb") * share_cols
    own_values = lax.dynamic_slice_in_dim(values, col_start, share_cols, 1)
    own_gain = lax.dynamic_slice_in_dim(post_gain, col_start, share_cols, 0)
    post_sq = over_copies(jnp.sum(share * share, axis=1), ("ra", "cb"))
    post_scale = lax.rsqrt(post_sq / dim_full + epsilon)
    mixed_part = (residual_scale * own_values + share * post_scale[:, None] * own_gain).astype(
        jnp.bfloat16
    )
    mixed = lax.all_gather(mixed_part, "cb", axis=1, tiled=True)
    return mixed[None]


def solution(mesh):
    in_specs = (
        P("dp", None, "ra"),
        P("ra"),
        P("ra", "cb"),
        P("ra", "cb"),
        P(None, "cb"),
        P(None, "cb"),
        P("cb", "ra"),
        P("ra"),
    )
    out_specs = P("dp", None, "ra")
    return jax.shard_map(local, mesh=mesh, in_specs=in_specs, out_specs=out_specs, check_vma=False)
```

profile of v0, /device:TPU:2, one launch (start us, length us, event | category | flops | bytes accessed | tf_op | source)
XLA Modules:
  0.0 356.9 jit_solution(16461781965745227600)
XLA Ops:
  6.5 0.0 copy-start
  6.5 1.2 copy.25
  7.7 1.5 fusion.3
  9.2 0.6 broadcast_in_dim.6
  9.9 15.2 %all-to-all-start.1 = ((f32[16,1,512]{2,1,0:T(1,128)}), f32[16,1,512]{2,1,0:T(1,128)S(1)}, u32[]{:S(2)}, u32[]{:S(2)}) async-start(f32[16,1,512]{2,1,0:T(1,128)} %broadcast_in_dim.6), calls=%async_computation.1 | async-start | bytes 65536 | tf_op jit(solution)/shard_map/all_to_all | solution.py:12
  25.1 2.5 copy.29
  27.6 10.0 %all-to-all-done.1 = f32[16,1,512]{2,1,0:T(1,128)S(1)} async-done(((f32[16,1,512]{2,1,0:T(1,128)}), f32[16,1,512]{2,1,0:T(1,128)S(1)}, u32[]{:S(2)}, u32[]{:S(2)}) %all-to-all-start.1) | async-done | bytes 32800 | tf_op jit(solution)/shard_map/all_to_all | solution.py:12
  37.6 3.7 %all-to-all-start.2 = ((bf16[256,16,176]{0,2,1:T(8,128)(2,1)}), bf16[256,16,176]{0,2,1:T(8,128)(2,1)S(1)}, u32[]{:S(2)}, u32[]{:S(2)}) async-start(bf16[256,16,176]{0,2,1:T(8,128)(2,1)} %bitcast.41), calls=%async_computation.2 | async-start | bytes 2883584 | tf_op jit(solution)/shard_map/all_to_all | solution.py:54
  41.3 0.0 all-gather.3.cloned.1.call-start
  41.4 0.7 all-gather.3.cloned.1.call-update
  42.1 2.5 copy.26
  44.6 72.1 %all-to-all-done.2 = bf16[256,16,176]{0,2,1:T(8,128)(2,1)S(1)} async-done(((bf16[256,16,176]{0,2,1:T(8,128)(2,1)}), bf16[256,16,176]{0,2,1:T(8,128)(2,1)S(1)}, u32[]{:S(2)}, u32[]{:S(2)}) %all-to-all-start.2) | async-done | bytes 1441824 | tf_op jit(solution)/shard_map/all_to_all | solution.py:54
  116.7 10.3 %all-to-all-start = ((bf16[256,16,176]{0,2,1:T(8,128)(2,1)}), bf16[256,16,176]{0,2,1:T(8,128)(2,1)}, u32[]{:S(2)}, u32[]{:S(2)}) async-start(bf16[256,16,176]{0,2,1:T(8,128)(2,1)} %bitcast.40), calls=%async_computation | async-start | bytes 2883584 | tf_op jit(solution)/shard_map/all_to_all | solution.py:53
  127.0 0.0 all-gather.5.cloned.1.call-start
  127.1 0.9 constant_dynamic-slice_fusion
  128.0 1.3 copy.36
  129.3 78.8 %all-to-all-done = bf16[256,16,176]{0,2,1:T(8,128)(2,1)} async-done(((bf16[256,16,176]{0,2,1:T(8,128)(2,1)}), bf16[256,16,176]{0,2,1:T(8,128)(2,1)}, u32[]{:S(2)}, u32[]{:S(2)}) %all-to-all-start) | async-done | bytes 1441824 | tf_op jit(solution)/shard_map/all_to_all | solution.py:53
  208.2 0.0 copy-start.2
  208.2 2.8 copy.35
  210.9 5.6 %all-gather.3.cloned.1.call-done = bf16[512,4096]{0,1:T(8,128)(2,1)} async-done(((bf16[512,256]{0,1:T(8,128)(2,1)}), bf16[512,4096]{0,1:T(8,128)(2,1)}) %all-gather.3.cloned.1.call-update) | async-done | bytes 4194320 | tf_op jit(solution)/shard_map/all_gather | solution.py:57
  216.5 0.0 copy-done.2
  216.5 0.0 copy-start.1
  216.5 0.0 copy-start.3
  216.5 3.3 fusion.1
  219.8 0.2 copy-done.1
  220.0 0.4 copy-done.3
  220.4 0.9 fusion
  221.3 0.3 fusion.14
  221.6 1.2 fusion.12
  222.8 0.0 all-gather.5.cloned.1.call-update
  222.8 72.5 %all-gather.5.cloned.1.call-done = bf16[2816,512]{1,0:T(8,128)(2,1)} async-done(((bf16[176,512]{1,0:T(8,128)(2,1)}), bf16[2816,512]{1,0:T(8,128)(2,1)}) %all-gather.5.cloned.1.call-update) | async-done | bytes 2883600 | tf_op jit(solution)/shard_map/all_gather | solution.py:70
  295.4 0.0 copy-done
  295.4 2.8 fusion.16
  298.1 0.0 copy-start.4
  298.1 12.2 %all_to_all.55 = f32[4,512,64]{1,2,0:T(8,128)S(1)} all-to-all(f32[4,512,64]{1,2,0:T(8,128)S(1)} %bitcast.45), channel_id=1, replica_groups=mesh['ra'=16,'cb'=4,'dp'=8] {'cb'}, dimensions={0} | all-to-all | bytes 1048576 | tf_op jit(solution)/shard_map/all_to_all | solution.py:29
  310.4 0.7 broadcast_in_dim.7
  311.2 9.4 %all-to-all-start.4 = ((f32[64,1,512]{2,1,0:T(1,128)}), f32[64,1,512]{2,1,0:T(1,128)S(1)}, u32[]{:S(2)}, u32[]{:S(2)}) async-start(f32[64,1,512]{2,1,0:T(1,128)} %broadcast_in_dim.7), calls=%async_computation.4 | async-start | bytes 262144 | tf_op jit(solution)/shard_map/all_to_all | solution.py:12
  320.6 0.1 convert_element_type.15
  320.6 0.0 copy-done.4
  320.7 0.1 dynamic_slice.15
  320.7 16.0 %all-to-all-done.4 = f32[64,1,512]{2,1,0:T(1,128)S(1)} async-done(((f32[64,1,512]{2,1,0:T(1,128)}), f32[64,1,512]{2,1,0:T(1,128)S(1)}, u32[]{:S(2)}, u32[]{:S(2)}) %all-to-all-start.4) | async-done | bytes 131104 | tf_op jit(solution)/shard_map/all_to_all | solution.py:12
  336.7 0.1 reduce_sum.49
  336.8 0.1 fusion.13
  336.9 12.3 %all_gather.11 = bf16[512,256]{0,1:T(8,128)(2,1)S(1)} all-gather(bf16[512,64]{0,1:T(8,128)(2,1)S(1)} %fusion.13), channel_id=1, replica_groups=mesh['ra'=16,'cb'=4,'dp'=8] {'cb'}, dimensions={1}, use_global_device_ids=true | all-gather | bytes 327680 | tf_op jit(solution)/shard_map/all_gather | solution.py:85
  349.2 0.8 copy.32
  (5 shorter events, 0.1 us)
Async XLA Ops:
  6.5 288.8 %copy-start = (bf16[2816,256]{1,0:T(8,128)(2,1)S(1)}, bf16[2816,256]{1,0:T(8,128)(2,1)}, u32[]{:S(2)}) copy-start(bf16[2816,256]{1,0:T(8,128)(2,1)} %param.14) | copy-start | bytes 4325380
  9.9 27.8 %all-to-all-start.1 = ((f32[16,1,512]{2,1,0:T(1,128)}), f32[16,1,512]{2,1,0:T(1,128)S(1)}, u32[]{:S(2)}, u32[]{:S(2)}) async-start(f32[16,1,512]{2,1,0:T(1,128)} %broadcast_in_dim.6), calls=%async_computation.1 | async-start | bytes 65536 | tf_op jit(solution)/shard_map/all_to_all | solution.py:12
  37.6 79.1 %all-to-all-start.2 = ((bf16[256,16,176]{0,2,1:T(8,128)(2,1)}), bf16[256,16,176]{0,2,1:T(8,128)(2,1)S(1)}, u32[]{:S(2)}, u32[]{:S(2)}) async-start(bf16[256,16,176]{0,2,1:T(8,128)(2,1)} %bitcast.41), calls=%async_computation.2 | async-start | bytes 2883584 | tf_op jit(solution)/shard_map/all_to_all | solution.py:54
  41.3 175.2 %all-gather.3.cloned.1.call-start = ((), (), s32[]{:S(2)}) async-start(), calls=%async_computation.5 | async-start | bytes 4456448 | tf_op jit(solution)/shard_map/all_gather | solution.py:57
  116.7 91.4 %all-to-all-start = ((bf16[256,16,176]{0,2,1:T(8,128)(2,1)}), bf16[256,16,176]{0,2,1:T(8,128)(2,1)}, u32[]{:S(2)}, u32[]{:S(2)}) async-start(bf16[256,16,176]{0,2,1:T(8,128)(2,1)} %bitcast.40), calls=%async_computation | async-start | bytes 2883584 | tf_op jit(solution)/shard_map/all_to_all | solution.py:53
  127.0 168.3 %all-gather.5.cloned.1.call-start = ((), (), s32[]{:S(2)}) async-start(), calls=%async_computation.6 | async-start | bytes 3063808 | tf_op jit(solution)/shard_map/all_gather | solution.py:70
  208.2 8.4 %copy-start.2 = (bf16[16,22,8,256]{3,2,0,1:T(8,128)(2,1)S(1)}, bf16[16,22,8,256]{3,2,0,1:T(8,128)(2,1)}, u32[]{:S(2)}) copy-start(bf16[16,22,8,256]{3,2,0,1:T(8,128)(2,1)} %copy.36) | copy-start | bytes 4325380
  216.5 3.4 copy-start.1
  216.5 3.9 %copy-start.3 = (bf16[16,22,8,256]{3,2,0,1:T(8,128)(2,1)S(1)}, bf16[16,22,8,256]{3,2,0,1:T(8,128)(2,1)}, u32[]{:S(2)}) copy-start(bf16[16,22,8,256]{3,2,0,1:T(8,128)(2,1)} %copy.35) | copy-start | bytes 4325380
  298.1 22.5 %copy-start.4 = (f32[256]{0:T(256)S(1)}, f32[256]{0:T(256)}, u32[]{:S(2)}) copy-start(f32[256]{0:T(256)} %param.15) | copy-start | bytes 3076
  311.2 25.6 %all-to-all-start.4 = ((f32[64,1,512]{2,1,0:T(1,128)}), f32[64,1,512]{2,1,0:T(1,128)S(1)}, u32[]{:S(2)}, u32[]{:S(2)}) async-start(f32[64,1,512]{2,1,0:T(1,128)} %broadcast_in_dim.7), calls=%async_computation.4 | async-start | bytes 262144 | tf_op jit(solution)/shard_map/all_to_all | solution.py:12
Sparse Core Ops, SparseCore 0:
  44.2 172.2 all-gather.2
  222.9 72.3 all-gather.4
where the time goes:
time: 357 us
  waiting for transfers between devices  256 us (72%)
  starting transfers between devices  38.7 us (11%)
  blocking collectives  24.5 us (7%)
  local copies, waits for them, and re-layouts  14.4 us (4%)
  between operations  13.5 us (4%)
  matrix products  6.94 us (2%)
    all_to_all x1, waiting for transfers between devices, local(): lax.all_to_all(w_gate, 'ra', split_axis=1, concat_axis=0, tiled=True)  78.8 us
    all_gather x1, waiting for transfers between devices, local(): lax.all_gather(hidden, 'ra', axis=0, tiled=True)  72.5 us
    all_to_all x1, waiting for transfers between devices, local(): lax.all_to_all(w_up, 'ra', split_axis=1, concat_axis=0, tiled=True)  72.1 us
    all_to_all x2, waiting for transfers between devices, from_everyone(): lax.all_to_all(jnp.broadcast_to(array[None], (count, *array.shape)), axis...  26 us
    all_to_all x2, starting transfers between devices, from_everyone(): lax.all_to_all(jnp.broadcast_to(array[None], (count, *array.shape)), axis...  24.6 us
    all_gather x1, blocking collectives, local(): mixed = lax.all_gather(mixed_part, 'cb', axis=1, tiled=True)  12.3 us
    all_to_all x1, blocking collectives, summed_on_arrival(): tiles = lax.all_to_all(split_up(array, dim, count), axis, 0, 0, tiled=True)  12.2 us
    all_to_all x1, starting transfers between devices, local(): lax.all_to_all(w_gate, 'ra', split_axis=1, concat_axis=0, tiled=True)  10.3 us
  transfers between devices with their start and end apart: 6, of which 6 were waited for; matrix products, arithmetic and copies ran while one was open for 3% of the time, Pallas kernels for 0%

commit v1 on v0

--- a/solution.py
+++ b/solution.py
@@ -66,8 +66,20 @@
     hidden = (
         jax.nn.gelu(convolve(gate_lin, taps_gate), approximate=True) * convolve(up_lin, taps_up)
     ).astype(jnp.bfloat16)
+
+    def _meet_floor(unit, device_axis):
+        return jnp.concatenate(
+            lax.all_to_all(
+                jnp.stack([unit] * lax.axis_size(device_axis), 0),
+                device_axis,
+                split_axis=0,
+                concat_axis=0,
+            ),
+            0,
+        )
+
     partial_value = lax.dot_general(
-        lax.all_gather(hidden, "ra", axis=0, tiled=True),
+        _meet_floor(hidden, "ra"),
         w_down,
         (((0,), (0,)), ((), ())),
         preferred_element_type=jnp.float32,

time: 357 us -> 421 us (1.18)
  waiting for transfers between devices: 256 us -> 305 us
  starting transfers between devices: 38.7 us -> 50.8 us
    all_to_all x0 -> x1, waiting for transfers between devices: none -> 120 us  [_meet_floor(): lax.all_to_all(jnp.stack([unit] * lax.axis_size(device_axis), 0), device_...]
    all_gather x1 -> x0, waiting for transfers between devices: 72.5 us -> none  [local(): lax.all_gather(hidden, 'ra', axis=0, tiled=True)]
    all_to_all x0 -> x1, starting transfers between devices: none -> 8.62 us  [_meet_floor(): lax.all_to_all(jnp.stack([unit] * lax.axis_size(device_axis), 0), device_...]
  transfers between devices with their start and end apart: 6 -> 6, of which waited for: 6 -> 6; matrix products, arithmetic and copies ran while one was open for 3% -> 2% of each run, Pallas kernels for 0% -> 0%
where the time goes in v1:
time: 421 us; the launch traced here: 420 us
  waiting for transfers between devices  305 us (72%)
  starting transfers between devices  50.8 us (12%)
  blocking collectives  25.3 us (6%)
  local copies, waits for them, and re-layouts  16.3 us (4%)
  between operations  13.6 us (3%)
  matrix products  6.44 us (2%)
    all_to_all x1, waiting for transfers between devices, _meet_floor(): lax.all_to_all(jnp.stack([unit] * lax.axis_size(device_axis), 0), device_...  120 us
    all_to_all x1, waiting for transfers between devices, local(): lax.all_to_all(w_gate, 'ra', split_axis=1, concat_axis=0, tiled=True)  78.8 us
    all_to_all x1, waiting for transfers between devices, local(): lax.all_to_all(w_up, 'ra', split_axis=1, concat_axis=0, tiled=True)  73.1 us
    all_to_all x2, starting transfers between devices, from_everyone(): lax.all_to_all(jnp.broadcast_to(array[None], (count, *array.shape)), axis...  28.1 us
    all_to_all x2, waiting for transfers between devices, from_everyone(): lax.all_to_all(jnp.broadcast_to(array[None], (count, *array.shape)), axis...  26.1 us
    all_to_all x1, blocking collectives, summed_on_arrival(): tiles = lax.all_to_all(split_up(array, dim, count), axis, 0, 0, tiled=True)  13 us
    all_gather x1, blocking collectives, local(): mixed = lax.all_gather(mixed_part, 'cb', axis=1, tiled=True)  12.3 us
    all_to_all x1, starting transfers between devices, local(): lax.all_to_all(w_gate, 'ra', split_axis=1, concat_axis=0, tiled=True)  10.2 us
  transfers between devices with their start and end apart: 6, of which 6 were waited for; matrix products, arithmetic and copies ran while one was open for 2% of the time, Pallas kernels for 0%

profile of v1, /device:TPU:2, one launch (start us, length us, event | category | flops | bytes accessed | tf_op | source)
XLA Modules:
  0.0 420.1 jit_solution(13928984655073143669)
XLA Ops:
  6.5 1.1 copy.29
  7.6 1.5 fusion.3
  9.1 0.6 broadcast_in_dim.6
  9.7 15.2 %all-to-all-start.1 = ((f32[16,1,512]{2,1,0:T(1,128)}), f32[16,1,512]{2,1,0:T(1,128)S(1)}, u32[]{:S(2)}, u32[]{:S(2)}) async-start(f32[16,1,512]{2,1,0:T(1,128)} %broadcast_in_dim.6), calls=%async_computation.1 | async-start | bytes 65536 | tf_op jit(solution)/shard_map/all_to_all | solution.py:12
  25.0 2.6 copy.33
  27.5 10.0 %all-to-all-done.1 = f32[16,1,512]{2,1,0:T(1,128)S(1)} async-done(((f32[16,1,512]{2,1,0:T(1,128)}), f32[16,1,512]{2,1,0:T(1,128)S(1)}, u32[]{:S(2)}, u32[]{:S(2)}) %all-to-all-start.1) | async-done | bytes 32800 | tf_op jit(solution)/shard_map/all_to_all | solution.py:12
  37.5 0.0 copy-start.3
  37.5 3.8 all-to-all-start.2
  41.4 0.0 all-gather.2.cloned.1.call-start
  41.4 0.7 all-gather.2.cloned.1.call-update
  42.1 0.0 copy-done.3
  42.1 1.6 copy.30
  43.7 73.1 %all-to-all-done.2 = bf16[256,16,176]{0,2,1:T(8,128)(2,1)S(1)} async-done(((bf16[256,16,176]{0,2,1:T(8,128)(2,1)}), bf16[256,16,176]{0,2,1:T(8,128)(2,1)S(1)}, u32[]{:S(2)}, u32[]{:S(2)}) %all-to-all-start.2) | async-done | bytes 1441824 | tf_op jit(solution)/shard_map/all_to_all | solution.py:54
  116.8 10.2 %all-to-all-start = ((bf16[256,16,176]{0,2,1:T(8,128)(2,1)}), bf16[256,16,176]{0,2,1:T(8,128)(2,1)S(1)}, u32[]{:S(2)}, u32[]{:S(2)}) async-start(bf16[256,16,176]{0,2,1:T(8,128)(2,1)} %bitcast.3), calls=%async_computation | async-start | bytes 2883584 | tf_op jit(solution)/shard_map/all_to_all | solution.py:53
  127.0 0.9 constant_dynamic-slice_fusion
  128.0 1.3 copy.41
  129.3 78.8 %all-to-all-done = bf16[256,16,176]{0,2,1:T(8,128)(2,1)S(1)} async-done(((bf16[256,16,176]{0,2,1:T(8,128)(2,1)}), bf16[256,16,176]{0,2,1:T(8,128)(2,1)S(1)}, u32[]{:S(2)}, u32[]{:S(2)}) %all-to-all-start) | async-done | bytes 1441824 | tf_op jit(solution)/shard_map/all_to_all | solution.py:53
  208.1 0.0 copy-start.1
  208.1 1.3 copy.40
  209.4 7.2 %all-gather.2.cloned.1.call-done = bf16[512,4096]{0,1:T(8,128)(2,1)} async-done(((bf16[512,256]{0,1:T(8,128)(2,1)}), bf16[512,4096]{0,1:T(8,128)(2,1)}) %all-gather.2.cloned.1.call-update) | async-done | bytes 4194320 | tf_op jit(solution)/shard_map/all_gather | solution.py:57
  216.6 0.0 copy-done.1
  216.6 0.0 copy-start
  216.6 0.0 copy-start.2
  216.6 3.3 fusion.1
  219.8 0.2 copy-done
  220.0 0.4 copy-done.2
  220.4 0.9 fusion
  221.4 0.3 fusion.14
  221.6 0.5 fusion.12
  222.1 1.9 stack.2
  224.0 8.6 %all-to-all-start.3 = ((bf16[16,176,512]{2,1,0:T(8,128)(2,1)}), bf16[16,176,512]{2,1,0:T(8,128)(2,1)S(1)}, u32[]{:S(2)}, u32[]{:S(2)}) async-start(bf16[16,176,512]{2,1,0:T(8,128)(2,1)} %stack.2), calls=%async_computation.3 | async-start | bytes 5767168 | tf_op jit(solution)/shard_map/all_to_all | solution.py:72
  232.6 2.5 copy.35
  235.1 119.6 %all-to-all-done.3 = bf16[16,176,512]{2,1,0:T(8,128)(2,1)S(1)} async-done(((bf16[16,176,512]{2,1,0:T(8,128)(2,1)}), bf16[16,176,512]{2,1,0:T(8,128)(2,1)S(1)}, u32[]{:S(2)}, u32[]{:S(2)}) %all-to-all-start.3) | async-done | bytes 2883616 | tf_op jit(solution)/shard_map/all_to_all | solution.py:72
  354.7 2.3 convolution_bitcast_fusion
  357.0 0.0 copy-start.4
  357.0 13.0 %all_to_all.60 = f32[4,512,64]{1,2,0:T(8,128)S(1)} all-to-all(f32[4,512,64]{1,2,0:T(8,128)S(1)} %convolution_bitcast_fusion), channel_id=1, replica_groups=mesh['ra'=16,'cb'=4,'dp'=8] {'cb'}, dimensions={0} | all-to-all | bytes 1048576 | tf_op jit(solution)/shard_map/all_to_all | solution.py:29
  370.1 0.7 broadcast_in_dim.7
  370.8 12.9 %all-to-all-start.5 = ((f32[64,1,512]{2,1,0:T(1,128)}), f32[64,1,512]{2,1,0:T(1,128)S(1)}, u32[]{:S(2)}, u32[]{:S(2)}) async-start(f32[64,1,512]{2,1,0:T(1,128)} %broadcast_in_dim.7), calls=%async_computation.5 | async-start | bytes 262144 | tf_op jit(solution)/shard_map/all_to_all | solution.py:12
  383.7 0.1 convert_element_type.15
  383.7 0.0 copy-done.4
  383.8 0.1 dynamic_slice.15
  383.8 16.1 %all-to-all-done.5 = f32[64,1,512]{2,1,0:T(1,128)S(1)} async-done(((f32[64,1,512]{2,1,0:T(1,128)}), f32[64,1,512]{2,1,0:T(1,128)S(1)}, u32[]{:S(2)}, u32[]{:S(2)}) %all-to-all-start.5) | async-done | bytes 131104 | tf_op jit(solution)/shard_map/all_to_all | solution.py:12
  400.0 0.1 reduce_sum.49
  400.1 0.1 fusion.13
  400.2 12.3 %all_gather.7 = bf16[512,256]{0,1:T(8,128)(2,1)S(1)} all-gather(bf16[512,64]{0,1:T(8,128)(2,1)S(1)} %fusion.13), channel_id=1, replica_groups=mesh['ra'=16,'cb'=4,'dp'=8] {'cb'}, dimensions={1}, use_global_device_ids=true | all-gather | bytes 327680 | tf_op jit(solution)/shard_map/all_gather | solution.py:97
  412.4 0.8 copy.37
  (5 shorter events, 0.1 us)
Async XLA Ops:
  9.7 27.8 %all-to-all-start.1 = ((f32[16,1,512]{2,1,0:T(1,128)}), f32[16,1,512]{2,1,0:T(1,128)S(1)}, u32[]{:S(2)}, u32[]{:S(2)}) async-start(f32[16,1,512]{2,1,0:T(1,128)} %broadcast_in_dim.6), calls=%async_computation.1 | async-start | bytes 65536 | tf_op jit(solution)/shard_map/all_to_all | solution.py:12
  37.5 4.6 %copy-start.3 = (bf16[256,2816]{1,0:T(8,128)(2,1)S(1)}, bf16[256,2816]{1,0:T(8,128)(2,1)}, u32[]{:S(2)}) copy-start(bf16[256,2816]{1,0:T(8,128)(2,1)} %param.10) | copy-start | bytes 4325380
  37.5 79.2 %all-to-all-start.2 = ((bf16[256,16,176]{0,2,1:T(8,128)(2,1)}), bf16[256,16,176]{0,2,1:T(8,128)(2,1)S(1)}, u32[]{:S(2)}, u32[]{:S(2)}) async-start(bf16[256,16,176]{0,2,1:T(8,128)(2,1)} %bitcast.9), calls=%async_computation.2 | async-start | bytes 2883584 | tf_op jit(solution)/shard_map/all_to_all | solution.py:54
  41.4 175.2 %all-gather.2.cloned.1.call-start = ((), (), s32[]{:S(2)}) async-start(), calls=%async_computation.6 | async-start | bytes 4456448 | tf_op jit(solution)/shard_map/all_gather | solution.py:57
  116.8 91.3 %all-to-all-start = ((bf16[256,16,176]{0,2,1:T(8,128)(2,1)}), bf16[256,16,176]{0,2,1:T(8,128)(2,1)S(1)}, u32[]{:S(2)}, u32[]{:S(2)}) async-start(bf16[256,16,176]{0,2,1:T(8,128)(2,1)} %bitcast.3), calls=%async_computation | async-start | bytes 2883584 | tf_op jit(solution)/shard_map/all_to_all | solution.py:53
  208.1 8.5 %copy-start.1 = (bf16[16,22,8,256]{3,2,0,1:T(8,128)(2,1)S(1)}, bf16[16,22,8,256]{3,2,0,1:T(8,128)(2,1)}, u32[]{:S(2)}) copy-start(bf16[16,22,8,256]{3,2,0,1:T(8,128)(2,1)} %copy.41) | copy-start | bytes 4325380
  216.6 3.4 copy-start
  216.6 3.9 copy-start.2
  224.0 130.7 %all-to-all-start.3 = ((bf16[16,176,512]{2,1,0:T(8,128)(2,1)}), bf16[16,176,512]{2,1,0:T(8,128)(2,1)S(1)}, u32[]{:S(2)}, u32[]{:S(2)}) async-start(bf16[16,176,512]{2,1,0:T(8,128)(2,1)} %stack.2), calls=%async_computation.3 | async-start | bytes 5767168 | tf_op jit(solution)/shard_map/all_to_all | solution.py:72
  357.0 26.8 %copy-start.4 = (f32[256]{0:T(256)S(1)}, f32[256]{0:T(256)}, u32[]{:S(2)}) copy-start(f32[256]{0:T(256)} %param.15) | copy-start | bytes 3076
  370.8 29.1 %all-to-all-start.5 = ((f32[64,1,512]{2,1,0:T(1,128)}), f32[64,1,512]{2,1,0:T(1,128)S(1)}, u32[]{:S(2)}, u32[]{:S(2)}) async-start(f32[64,1,512]{2,1,0:T(1,128)} %broadcast_in_dim.7), calls=%async_computation.5 | async-start | bytes 262144 | tf_op jit(solution)/shard_map/all_to_all | solution.py:12
Sparse Core Ops, SparseCore 0:
  44.3 172.2 all-gather.1
